TPU v7x, 32 devices: a whole 2x2x4 slice. The times are simulated.
32 devices in a mesh: rep: 2 (over x), fs: 8 (over z, y), tp: 2 (over core).
Axes of the slice: x: 2, y: 2, z: 4, core: 2. Of those that a mesh axis runs over, the one named last changes fastest.
Arguments:
- tokens: bfloat16 [8192, 2048], P(('rep', 'fs')), may hold values from -6 to 6
- mix_gain: bfloat16 [2048], replicated, may hold values from 0.099609375 to 1.8984375
- value_weight: bfloat16 [2048, 1536], P('fs', 'tp'), may hold values from -0.125 to 0.125
- outer_gate_weight: bfloat16 [2048, 1536], P('fs', 'tp'), may hold values from -0.125 to 0.125
- inner_gate_weight: bfloat16 [2048, 1536], P('fs', 'tp'), may hold values from -0.125 to 0.125
- conv_taps: bfloat16 [3, 1536], P(None, 'tp'), may hold values from -3 to 3
- mix_out_weight: bfloat16 [1536, 2048], P('tp', 'fs'), may hold values from -0.15625 to 0.15625
- ffn_gain: bfloat16 [2048], replicated, may hold values from 0.099609375 to 1.8984375
- gate_weight: bfloat16 [2048, 4096], P('fs', 'tp'), may hold values from -0.125 to 0.125
- up_weight: bfloat16 [2048, 4096], P('fs', 'tp'), may hold values from -0.125 to 0.125
- down_weight: bfloat16 [4096, 2048], P('tp', 'fs'), may hold values from -0.09375 to 0.09375
Outputs:
- layer_out: bfloat16 [8192, 2048], P(('rep', 'fs'))
All inputs are finite; a program needn't handle non-finite values.
Results may differ from a plain program's by a relative error of at most 0.02.
Values may be sent and summed in bfloat16 or wider, within the bound.
A program may use at most 128 MiB of HBM per device.

v0:
```python
import jax
import jax.numpy as jnp
from jax import lax
from jax.sharding import PartitionSpec as P

SEQ_GRP = 2


EPS = 1e-05


def rms_norm(values, gain):
    floats = values.astype(jnp.float32)
    scaled = floats * lax.rsqrt(jnp.mean(floats * floats, axis=-1, keepdims=True) + EPS)
    return (scaled * gain.astype(jnp.float32)).astype(jnp.bfloat16)


def short_conv(value_proj, outer_proj, inner_proj, conv_taps, seq_len):
    mixed_in = inner_proj.astype(jnp.float32) * value_proj.astype(jnp.float32)
    count_rows = mixed_in.shape[0]
    position = (jnp.arange(count_rows, dtype=jnp.int32) % seq_len)[:, None]
    zero_row = jnp.zeros((1, mixed_in.shape[1]), jnp.float32)
    back_one = jnp.where(position >= 1, jnp.concatenate([zero_row, mixed_in[:-1]], axis=0), 0.0)
    back_two = jnp.where(
        position >= 2, jnp.concatenate([zero_row, zero_row, mixed_in[:-2]], axis=0), 0.0
    )
    taps = conv_taps.astype(jnp.float32)
    convolved = taps[0] * back_two + taps[1] * back_one + taps[2] * mixed_in
    return (outer_proj.astype(jnp.float32) * convolved).astype(jnp.bfloat16)


def local(
    tokens,
    mix_gain,
    value_weight,
    outer_gate_weight,
    inner_gate_weight,
    conv_taps,
    mix_out_weight,
    ffn_gain,
    gate_weight,
    up_weight,
    down_weight,
):
    row_count = tokens.shape[0]
    share = row_count // lax.axis_size("tp")
    seq_len = row_count // SEQ_GRP
    own_rows = lax.dynamic_slice_in_dim(tokens, lax.axis_index("tp") * share, share, 0).astype(
        jnp.float32
    )
    normed = rms_norm(tokens, mix_gain)
    value_full, outer_full, inner_full, mix_out_full, gate_full, up_full, down_full = (
        lax.all_gather(value_weight, "fs", axis=0, tiled=True),
        lax.all_gather(outer_gate_weight, "fs", axis=0, tiled=True),
        lax.all_gather(inner_gate_weight, "fs", axis=0, tiled=True),
        lax.all_gather(mix_out_weight, "fs", axis=1, tiled=True),
        lax.all_gather(gate_weight, "fs", axis=0, tiled=True),
        lax.all_gather(up_weight, "fs", axis=0, tiled=True),
        lax.all_gather(down_weight, "fs", axis=1, tiled=True),
    )
    value_proj = jnp.dot(normed, value_full, preferred_element_type=jnp.float32).astype(
        jnp.bfloat16
    )
    outer_proj = jnp.dot(normed, outer_full, preferred_element_type=jnp.float32).astype(
        jnp.bfloat16
    )
    inner_proj = jnp.dot(normed, inner_full, preferred_element_type=jnp.float32).astype(
        jnp.bfloat16
    )
    mixed = short_conv(value_proj, outer_proj, inner_proj, conv_taps, seq_len)
    picked = mixed
    mix_total = lax.psum_scatter(
        jnp.dot(picked, mix_out_full, preferred_element_type=jnp.float32).astype(jnp.bfloat16),
        "tp",
        scatter_dimension=0,
        tiled=True,
    ).astype(jnp.float32)
    after_mix = (own_rows + mix_total).astype(jnp.bfloat16)
    normed_two = rms_norm(after_mix, ffn_gain)
    block_rows = lax.all_gather(normed_two, "tp", axis=0, tiled=True)
    gate_proj = jnp.dot(block_rows, gate_full, preferred_element_type=jnp.float32)
    up_proj = jnp.dot(block_rows, up_full, preferred_element_type=jnp.float32)
    hidden = (jax.nn.silu(gate_proj) * up_proj).astype(jnp.bfloat16)
    picked = hidden
    ffn_total = lax.psum_scatter(
        jnp.dot(picked, down_full, preferred_element_type=jnp.float32).astype(jnp.bfloat16),
        "tp",
        scatter_dimension=0,
        tiled=True,
    ).astype(jnp.float32)
    finished = (after_mix.astype(jnp.float32) + ffn_total).astype(jnp.bfloat16)
    return lax.all_gather(finished, "tp", axis=0, tiled=True)


def solution(mesh):
    placed = (
        P(("rep", "fs"), None),
        P(),
        P("fs", "tp"),
        P("fs", "tp"),
        P("fs", "tp"),
        P(None, "tp"),
        P("tp", "fs"),
        P(),
        P("fs", "tp"),
        P("fs", "tp"),
        P("tp", "fs"),
    )
    return jax.shard_map(
        local, mesh=mesh, in_specs=placed, out_specs=P(("rep", "fs"), None), check_vma=False
    )
```

profile of v0, /device:TPU:0, one launch (start us, length us, event | category | flops | bytes accessed | tf_op | source)
XLA Modules:
  0.0 718.0 jit_solution(16249208888733937228)
XLA Ops:
  6.5 0.7 all-gather.14.cloned.1.call-update
  7.3 0.7 all-gather.12.cloned.1.call-update
  10.8 2.1 fusion
  12.9 59.4 %all-gather.14.cloned.1.call-done = bf16[2048,768]{1,0:T(8,128)(2,1)} async-done(((bf16[256,768]{1,0:T(8,128)(2,1)}), bf16[2048,768]{1,0:T(8,128)(2,1)}) %all-gather.14.cloned.1.call-update) | async-done | bytes 3145744 | tf_op jit(solution)/shard_map/all_gather | solution.py:53
  72.3 3.7 convolution_convert_fusion.2
  76.0 57.2 %all-gather.12.cloned.1.call-done = bf16[2048,768]{1,0:T(8,128)(2,1)} async-done(((bf16[256,768]{1,0:T(8,128)(2,1)}), bf16[2048,768]{1,0:T(8,128)(2,1)}) %all-gather.12.cloned.1.call-update) | async-done | bytes 3145744 | tf_op jit(solution)/shard_map/all_gather | solution.py:55
  133.2 4.9 convert_multiply_fusion.4
  138.1 56.0 %all-gather.10.cloned.1.call-done = bf16[2048,768]{1,0:T(8,128)(2,1)} async-done(((bf16[256,768]{1,0:T(8,128)(2,1)}), bf16[2048,768]{1,0:T(8,128)(2,1)}) %all-gather.10.cloned.1.call-update) | async-done | bytes 3145744 | tf_op jit(solution)/shard_map/all_gather | solution.py:54
  194.1 63.2 %all-gather.16.cloned.1.call-done = bf16[768,2048]{1,0:T(8,128)(2,1)} async-done(((bf16[768,256]{1,0:T(8,128)(2,1)}), bf16[768,2048]{1,0:T(8,128)(2,1)}) %all-gather.16.cloned.1.call-update) | async-done | bytes 3145744 | tf_op jit(solution)/shard_map/all_gather | solution.py:56
  257.3 9.8 %convolution_convert_fusion.1 = bf16[512,2048]{1,0:T(8,128)(2,1)} fusion(bf16[768,2048]{1,0:T(8,128)(2,1)} %all-gather.16.cloned.1.call-done, f32[512,768]{1,0:T(8,128)} %convert_multiply_fusion.4, f32[511,768]{1,0:T(8,128)} %bitcast.20, f32[510,768]{1,0:T(8,128)} %bitcast.21, bf16[2048,768]{1,0:T(8,128)(2,1)} %all-gather.10.cloned.1.call-done, ...), kind=kOutput, calls=%fused_computation.10 | convolution fusion | flops 3230793728 | bytes 15215616 | tf_op jit(solution)/shard_map/dot_general | solution.py:73
  267.8 7.4 %reduce-scatter.3.cloned.1.call-done = bf16[256,2048]{1,0:T(8,128)(2,1)} async-done(((bf16[512,2048]{1,0:T(8,128)(2,1)}), bf16[256,2048]{1,0:T(8,128)(2,1)}) %reduce-scatter.3.cloned.1.call-update) | async-done | bytes 1048592 | tf_op jit(solution)/shard_map/reduce_scatter | solution.py:72
  275.3 1.7 fusion.3
  277.0 1.3 fusion.5
  278.4 0.7 all-gather.20.cloned.1.call-update
  280.8 9.6 %all-gather.18.cloned.1.call-done = bf16[512,2048]{1,0:T(8,128)(2,1)} async-done(((bf16[256,2048]{1,0:T(8,128)(2,1)}), bf16[512,2048]{1,0:T(8,128)(2,1)}) %all-gather.18.cloned.1.call-update) | async-done | bytes 2097168 | tf_op jit(solution)/shard_map/all_gather | solution.py:80
  290.4 127.8 %all-gather.20.cloned.1.call-done = bf16[2048,2048]{1,0:T(8,128)(2,1)} async-done(((bf16[256,2048]{1,0:T(8,128)(2,1)}), bf16[2048,2048]{1,0:T(8,128)(2,1)}) %all-gather.20.cloned.1.call-update) | async-done | bytes 8388624 | tf_op jit(solution)/shard_map/all_gather | solution.py:57
  418.2 10.5 %fusion.17 = f32[512,2048]{1,0:T(8,128)} fusion(bf16[512,2048]{1,0:T(8,128)(2,1)} %all-gather.18.cloned.1.call-done, bf16[2048,2048]{1,0:T(8,128)(2,1)} %all-gather.20.cloned.1.call-done), kind=kOutput, calls=%fused_computation.34 | convolution fusion | flops 4294967296 | bytes 14680064 | tf_op jit(solution)/shard_map/dot_general | solution.py:81
  428.6 114.3 %all-gather.22.cloned.1.call-done = bf16[2048,2048]{1,0:T(8,128)(2,1)} async-done(((bf16[256,2048]{1,0:T(8,128)(2,1)}), bf16[2048,2048]{1,0:T(8,128)(2,1)}) %all-gather.22.cloned.1.call-update) | async-done | bytes 8388624 | tf_op jit(solution)/shard_map/all_gather | solution.py:58
  543.0 125.2 %all-gather.24.cloned.1.call-done = bf16[2048,2048]{1,0:T(8,128)(2,1)} async-done(((bf16[2048,256]{1,0:T(8,128)(2,1)}), bf16[2048,2048]{1,0:T(8,128)(2,1)}) %all-gather.24.cloned.1.call-update) | async-done | bytes 8388624 | tf_op jit(solution)/shard_map/all_gather | solution.py:59
  668.2 17.4 %convolution_convert_fusion = bf16[512,2048]{1,0:T(8,128)(2,1)} fusion(bf16[2048,2048]{1,0:T(8,128)(2,1)} %all-gather.24.cloned.1.call-done, f32[512,2048]{1,0:T(8,128)} %fusion.17, bf16[512,2048]{1,0:T(8,128)(2,1)S(1)} %copy-done.2, bf16[2048,2048]{1,0:T(8,128)(2,1)} %all-gather.22.cloned.1.call-done), kind=kOutput, calls=%fused_computation.9 | convolution fusion | flops 8597274624 | bytes 25165824 | tf_op jit(solution)/shard_map/dot_general | solution.py:86
  685.7 8.0 %reduce-scatter.5.cloned.1.call-done = bf16[256,2048]{1,0:T(8,128)(2,1)} async-done(((bf16[512,2048]{1,0:T(8,128)(2,1)}), bf16[256,2048]{1,0:T(8,128)(2,1)}) %reduce-scatter.5.cloned.1.call-update) | async-done | bytes 1048592 | tf_op jit(solution)/shard_map/reduce_scatter | solution.py:85
  693.7 2.6 fusion.6
  696.3 12.0 %all-gather.26.cloned.1.call-done = bf16[512,2048]{1,0:T(8,128)(2,1)} async-done(((bf16[256,2048]{1,0:T(8,128)(2,1)}), bf16[512,2048]{1,0:T(8,128)(2,1)}) %all-gather.26.cloned.1.call-update) | async-done | bytes 2097168 | tf_op jit(solution)/shard_map/all_gather | solution.py:92
  708.3 3.2 copy.13
  (32 shorter events, 5.3 us)
Async XLA Ops:
  6.5 65.8 %copy-start = (bf16[512,2048]{1,0:T(8,128)(2,1)S(1)}, bf16[512,2048]{1,0:T(8,128)(2,1)}, u32[]{:S(2)}) copy-start(bf16[512,2048]{1,0:T(8,128)(2,1)} %param.11) | copy-start | bytes 6291460
  6.5 65.8 %all-gather.14.cloned.1.call-start = ((), (), s32[]{:S(2)}) async-start(), calls=%async_computation.4 | async-start | bytes 3538944 | tf_op jit(solution)/shard_map/all_gather | solution.py:53
  7.3 125.9 %all-gather.12.cloned.1.call-start = ((), (), s32[]{:S(2)}) async-start(), calls=%async_computation.3 | async-start | bytes 3538944 | tf_op jit(solution)/shard_map/all_gather | solution.py:55
  8.0 186.1 %all-gather.10.cloned.1.call-start = ((), (), s32[]{:S(2)}) async-start(), calls=%async_computation.2 | async-start | bytes 3538944 | tf_op jit(solution)/shard_map/all_gather | solution.py:54
  8.7 248.6 %all-gather.16.cloned.1.call-start = ((), (), s32[]{:S(2)}) async-start(), calls=%async_computation.5 | async-start | bytes 3538944 | tf_op jit(solution)/shard_map/all_gather | solution.py:56
  9.3 266.0 %reduce-scatter.3.cloned.1.call-start = ((), (), s32[]{:S(2)}) async-start(), calls=%async_computation.6 | async-start | bytes 3145728 | tf_op jit(solution)/shard_map/reduce_scatter | solution.py:72
  267.2 0.7 copy-start.1
  267.2 23.2 %all-gather.18.cloned.1.call-start = ((), (), s32[]{:S(2)}) async-start(), calls=%async_computation.7 | async-start | bytes 3145728 | tf_op jit(solution)/shard_map/all_gather | solution.py:80
  278.3 139.8 %all-gather.20.cloned.1.call-start = ((), (), s32[]{:S(2)}) async-start(), calls=%async_computation.8 | async-start | bytes 9437184 | tf_op jit(solution)/shard_map/all_gather | solution.py:57
  279.1 263.9 %all-gather.22.cloned.1.call-start = ((), (), s32[]{:S(2)}) async-start(), calls=%async_computation.9 | async-start | bytes 9437184 | tf_op jit(solution)/shard_map/all_gather | solution.py:58
  279.8 388.3 %all-gather.24.cloned.1.call-start = ((), (), s32[]{:S(2)}) async-start(), calls=%async_computation.10 | async-start | bytes 9437184 | tf_op jit(solution)/shard_map/all_gather | solution.py:59
  280.6 413.1 %reduce-scatter.5.cloned.1.call-start = ((), (), s32[]{:S(2)}) async-start(), calls=%async_computation.11 | async-start | bytes 3145728 | tf_op jit(solution)/shard_map/reduce_scatter | solution.py:85
  290.4 377.8 %copy-start.2 = (bf16[512,2048]{1,0:T(8,128)(2,1)S(1)}, bf16[512,2048]{1,0:T(8,128)(2,1)}, u32[]{:S(2)}) copy-start(bf16[512,2048]{1,0:T(8,128)(2,1)} %all-gather.18.cloned.1.call-done) | copy-start | bytes 6291460
  685.6 22.7 %all-gather.26.cloned.1.call-start = ((), (), s32[]{:S(2)}) async-start(), calls=%async_computation.12 | async-start | bytes 3145728 | tf_op jit(solution)/shard_map/all_gather | solution.py:92
Sparse Core Ops, SparseCore 0:
  9.5 62.7 all-gather.13
  74.5 58.6 all-gather.11
  135.4 58.6 all-gather.9
  196.0 61.3 all-gather.15
  267.3 7.9 reduce-scatter.2
  278.5 11.8 all-gather.17
  292.5 125.6 all-gather.19
  420.3 122.6 all-gather.21
  545.0 123.1 all-gather.23
  685.7 7.9 reduce-scatter.4
  696.4 11.8 all-gather.25
where the time goes:
time: 718 us
  waiting for transfers between devices  645 us (90%)
  matrix products  46.3 us (6%)
  between operations  13.3 us (2%)
  other arithmetic  9.09 us (1%)
    all_gather x1, waiting for transfers between devices, local(): lax.all_gather(gate_weight, 'fs', axis=0, tiled=True)  128 us
    all_gather x1, waiting for transfers between devices, local(): lax.all_gather(down_weight, 'fs', axis=1, tiled=True)  125 us
    all_gather x1, waiting for transfers between devices, local(): lax.all_gather(up_weight, 'fs', axis=0, tiled=True)  114 us
    all_gather x1, waiting for transfers between devices, local(): lax.all_gather(mix_out_weight, 'fs', axis=1, tiled=True)  63.2 us
    all_gather x1, waiting for transfers between devices, local(): lax.all_gather(value_weight, 'fs', axis=0, tiled=True)  59.4 us
    all_gather x1, waiting for transfers between devices, local(): lax.all_gather(inner_gate_weight, 'fs', axis=0, tiled=True)  57.2 us
    all_gather x1, waiting for transfers between devices, local(): lax.all_gather(outer_gate_weight, 'fs', axis=0, tiled=True)  56 us
    dot_general x1, matrix products, local(): jnp.dot(picked, down_full, preferred_element_type=jnp.float32)  17.4 us
  transfers between devices with their start and end apart: 11, of which 11 were waited for; matrix products, arithmetic and copies ran while one was open for 3% of the time, Pallas kernels for 0%

commit v1 on v0

v1 whole, which is shorter than its diff:
```python
import jax
import jax.numpy as jnp
from jax import lax
from jax.sharding import PartitionSpec as P

SEQ_GRP = 2


EPS = 1e-05


def rms_norm(values, gain):
    floats = values.astype(jnp.float32)
    scaled = floats * lax.rsqrt(jnp.mean(floats * floats, axis=-1, keepdims=True) + EPS)
    return (scaled * gain.astype(jnp.float32)).astype(jnp.bfloat16)


def short_conv(value_proj, outer_proj, inner_proj, conv_taps, seq_len):
    mixed_in = inner_proj.astype(jnp.float32) * value_proj.astype(jnp.float32)
    count_rows = mixed_in.shape[0]
    position = (jnp.arange(count_rows, dtype=jnp.int32) % seq_len)[:, None]
    zero_row = jnp.zeros((1, mixed_in.shape[1]), jnp.float32)
    back_one = jnp.where(position >= 1, jnp.concatenate([zero_row, mixed_in[:-1]], axis=0), 0.0)
    back_two = jnp.where(
        position >= 2, jnp.concatenate([zero_row, zero_row, mixed_in[:-2]], axis=0), 0.0
    )
    taps = conv_taps.astype(jnp.float32)
    convolved = taps[0] * back_two + taps[1] * back_one + taps[2] * mixed_in
    return (outer_proj.astype(jnp.float32) * convolved).astype(jnp.bfloat16)


def shifted(values, axis, step):
    size = lax.axis_size(axis)
    return lax.ppermute(values, axis, [(i, (i + step) % size) for i in range(size)])


def spread(block, axis):
    size, me, rows = lax.axis_size(axis), lax.axis_index(axis), block.shape[0]
    if size == 2:
        other = shifted(block, axis, 1)
        first = me == 0
        return jnp.concatenate([jnp.where(first, block, other), jnp.where(first, other, block)])
    whole = jnp.zeros((size * rows,) + block.shape[1:], block.dtype)
    for step in range(size):
        piece = block if step == 0 else shifted(block, axis, step)
        whole = lax.dynamic_update_slice_in_dim(whole, piece, (me - step) % size * rows, 0)
    return whole


def by_rep(block):
    return [block] + [shifted(block, "rep", step) for step in range(1, lax.axis_size("rep"))]


def group_rows(share_block):
    return jnp.concatenate([spread(block, "tp") for block in by_rep(share_block)])


def reduce_rows(partial, share):
    n_tp, tp, n_rep = lax.axis_size("tp"), lax.axis_index("tp"), lax.axis_size("rep")
    groups = partial.reshape(n_rep, n_tp, share, partial.shape[1])

    def chunk(step):
        return lax.dynamic_index_in_dim(groups, (tp + step) % n_tp, 1, keepdims=False)

    total = chunk(0).astype(jnp.float32)
    for step in range(1, n_tp):
        total = total + shifted(chunk(step), "tp", step).astype(jnp.float32)
    own = total[0]
    for step in range(1, n_rep):
        own = own + shifted(total[step].astype(jnp.bfloat16), "rep", -step).astype(jnp.float32)
    return own


def local(
    tokens,
    mix_gain,
    value_weight,
    outer_gate_weight,
    inner_gate_weight,
    conv_taps,
    mix_out_weight,
    ffn_gain,
    gate_weight,
    up_weight,
    down_weight,
):
    row_count = tokens.shape[0]
    share = row_count // lax.axis_size("tp")
    seq_len = row_count // SEQ_GRP
    n_rep, rep = lax.axis_size("rep"), lax.axis_index("rep")

    def part(array, axis):
        size = array.shape[axis] // n_rep
        return lax.dynamic_slice_in_dim(array, rep * size, size, axis)

    own_tokens = lax.dynamic_slice_in_dim(tokens, lax.axis_index("tp") * share, share, 0)
    conv_in = jnp.concatenate(
        [part(w, 1) for w in (value_weight, outer_gate_weight, inner_gate_weight)], axis=1
    )
    conv_full = lax.all_gather(conv_in, "fs", axis=0, tiled=True)
    mix_out_full = lax.all_gather(part(mix_out_weight, 0), "fs", axis=1, tiled=True)
    ffn_in = jnp.concatenate([part(w, 1) for w in (gate_weight, up_weight)], axis=1)
    ffn_full = lax.all_gather(ffn_in, "fs", axis=0, tiled=True)
    down_full = lax.all_gather(part(down_weight, 0), "fs", axis=1, tiled=True)

    normed = rms_norm(tokens, mix_gain)
    own_normed = lax.dynamic_slice_in_dim(normed, lax.axis_index("tp") * share, share, 0)
    rows = jnp.concatenate([normed] + [spread(b, "tp") for b in by_rep(own_normed)[1:]])
    proj = jnp.dot(rows, conv_full, preferred_element_type=jnp.float32).astype(jnp.bfloat16)
    value_proj, outer_proj, inner_proj = jnp.split(proj, 3, axis=1)
    mixed = short_conv(value_proj, outer_proj, inner_proj, part(conv_taps, 1), seq_len)
    mix_total = reduce_rows(
        jnp.dot(mixed, mix_out_full, preferred_element_type=jnp.float32).astype(jnp.bfloat16), share
    )
    after_mix = (own_tokens.astype(jnp.float32) + mix_total).astype(jnp.bfloat16)
    block_rows = group_rows(rms_norm(after_mix, ffn_gain))
    both = jnp.dot(block_rows, ffn_full, preferred_element_type=jnp.float32)
    gate_proj, up_proj = jnp.split(both, 2, axis=1)
    hidden = (jax.nn.silu(gate_proj) * up_proj).astype(jnp.bfloat16)
    ffn_total = reduce_rows(
        jnp.dot(hidden, down_full, preferred_element_type=jnp.float32).astype(jnp.bfloat16), share
    )
    finished = (after_mix.astype(jnp.float32) + ffn_total).astype(jnp.bfloat16)
    return spread(finished, "tp")


def solution(mesh):
    placed = (
        P(("rep", "fs"), None),
        P(),
        P("fs", "tp"),
        P("fs", "tp"),
        P("fs", "tp"),
        P(None, "tp"),
        P("tp", "fs"),
        P(),
        P("fs", "tp"),
        P("fs", "tp"),
        P("tp", "fs"),
    )
    return jax.shard_map(
        local, mesh=mesh, in_specs=placed, out_specs=P(("rep", "fs"), None), check_vma=False
    )
```

time: 718 us -> 388 us (0.54)
  waiting for transfers between devices: 645 us -> 299 us
  local copies, waits for them, and re-layouts: 3.81 us -> 12 us
  other arithmetic: 9.09 us -> 16.5 us
  starting transfers between devices: 0.57 us -> 7.97 us
  matrix products: 46.3 us -> 38.9 us
    all_gather x9 -> x4, waiting for transfers between devices: 625 us -> 190 us  [the longest x1 60.9 us: local(): down_full = lax.all_gather(part(down_weight, 0), 'fs', axis=1, tiled=True)]
    ppermute x0 -> x10, waiting for transfers between devices: none -> 109 us  [shifted(): lax.ppermute(values, axis, [(i, (i + step) % size) for i in range(size)])]
    reduce_scatter x2 -> x0, waiting for transfers between devices: 15.5 us -> none  [the longest x1 8.05 us: local(): lax.psum_scatter(jnp.dot(picked, down_full, preferred_element_type=jnp.fl...]
    ppermute x0 -> x10, starting transfers between devices: none -> 7.84 us  [shifted(): lax.ppermute(values, axis, [(i, (i + step) % size) for i in range(size)])]
    dot_general x5 -> x4, matrix products: 46.3 us -> 38.9 us  [the longest x1 13.8 us: local(): both = jnp.dot(block_rows, ffn_full, preferred_element_type=jnp.float32)]
  transfers between devices with their start and end apart: 11 -> 14, of which waited for: 11 -> 13; matrix products, arithmetic and copies ran while one was open for 3% -> 12% of each run, Pallas kernels for 0% -> 0%
where the time goes in v1:
time: 388 us; the launch traced here: 387 us
  waiting for transfers between devices  299 us (77%)
  matrix products  38.9 us (10%)
  other arithmetic  16.5 us (4%)
  between operations  13.4 us (3%)
  local copies, waits for them, and re-layouts  12 us (3%)
  starting transfers between devices  7.97 us (2%)
    ppermute x10, waiting for transfers between devices, shifted(): lax.ppermute(values, axis, [(i, (i + step) % size) for i in range(size)])  109 us
    all_gather x1, waiting for transfers between devices, local(): down_full = lax.all_gather(part(down_weight, 0), 'fs', axis=1, tiled=True)  60.9 us
    all_gather x1, waiting for transfers between devices, local(): ffn_full = lax.all_gather(ffn_in, 'fs', axis=0, tiled=True)  52.6 us
    all_gather x1, waiting for transfers between devices, local(): conv_full = lax.all_gather(conv_in, 'fs', axis=0, tiled=True)  43.9 us
    all_gather x1, waiting for transfers between devices, local(): lax.all_gather(part(mix_out_weight, 0), 'fs', axis=1, tiled=True)  32.2 us
    dot_general x1, matrix products, local(): both = jnp.dot(block_rows, ffn_full, preferred_element_type=jnp.float32)  13.8 us
    dot_general x1, matrix products, local(): jnp.dot(rows, conv_full, preferred_element_type=jnp.float32)  9.83 us
    dot_general x1, matrix products, local(): jnp.dot(hidden, down_full, preferred_element_type=jnp.float32)  9.19 us
  transfers between devices with their start and end apart: 14, of which 13 were waited for; matrix products, arithmetic and copies ran while one was open for 12% of the time, Pallas kernels for 0%

profile of v1, /device:TPU:0, one launch (start us, length us, event | category | flops | bytes accessed | tf_op | source)
XLA Modules:
  0.0 387.4 jit_solution(13555058826445362777)
XLA Ops:
  15.6 3.0 collective-permute-start
  18.6 23.3 %collective-permute-done = bf16[256,2048]{1,0:T(8,128)(2,1)} collective-permute-done((bf16[256,2048]{1,0:T(8,128)(2,1)S(1)}, bf16[256,2048]{1,0:T(8,128)(2,1)}, u32[]{:S(2)}, u32[]{:S(2)}) %collective-permute-start) | collective-permute-done | bytes 1048608 | tf_op jit(solution)/shard_map/ppermute | solution.py:34
  41.9 2.9 collective-permute-done.1
  44.9 3.0 broadcast_select_fusion.7
  47.9 43.9 %all-gather.5.cloned.1.call-done = bf16[2048,1152]{1,0:T(8,128)(2,1)} async-done(((bf16[256,1152]{1,0:T(8,128)(2,1)}), bf16[2048,1152]{1,0:T(8,128)(2,1)}) %all-gather.5.cloned.1.call-update) | async-done | bytes 4718608 | tf_op jit(solution)/shard_map/all_gather | solution.py:100
  91.8 9.8 %fusion.18 = bf16[1024,1152]{1,0:T(8,128)(2,1)S(1)} fusion(bf16[2048,1152]{1,0:T(8,128)(2,1)} %all-gather.5.cloned.1.call-done, bf16[256,2048]{1,0:T(8,128)(2,1)} %get-tuple-element.17, bf16[256,2048]{1,0:T(8,128)(2,1)} %get-tuple-element.16, bf16[512,2048]{1,0:T(8,128)(2,1)} %copy-done.3), kind=kOutput, calls=%fused_computation.24 | convolution fusion | flops 4845600768 | bytes 11272192 | tf_op jit(solution)/shard_map/dot_general | solution.py:109
  104.4 32.2 %all-gather.7.cloned.1.call-done = bf16[384,2048]{1,0:T(8,128)(2,1)} async-done(((bf16[384,256]{1,0:T(8,128)(2,1)}), bf16[384,2048]{1,0:T(8,128)(2,1)}) %all-gather.7.cloned.1.call-update) | async-done | bytes 1572880 | tf_op jit(solution)/shard_map/all_gather | solution.py:101
  136.6 6.0 %convolution_convert_fusion = bf16[1024,2048]{1,0:T(8,128)(2,1)S(1)} fusion(bf16[384,2048]{1,0:T(8,128)(2,1)} %all-gather.7.cloned.1.call-done, f32[1023,384]{1,0:T(8,128)} %bitcast.45, f32[1022,384]{1,0:T(8,128)} %bitcast.46, bf16[1024,1152]{1,0:T(8,128)(2,1)} %copy-done.5, f32[384]{0:T(512)S(1)} %get-tuple-element.6, f32[384]{0:T(512)S(1)} %get-tuple-element.7, ...), kind=kOutput, calls=%fused_computation.23 | convolution fusion | flops 1617821696 | bytes 11274240 | tf_op jit(solution)/shard_map/dot_general | solution.py:113
  142.7 2.0 copy-done.4
  144.7 1.6 dynamic-slice_bitcast_fusion.1
  147.1 3.6 collective-permute-done.2
  150.7 3.0 convert_add_fusion.1
  155.5 23.7 %collective-permute-done.3 = bf16[256,2048]{1,0:T(8,128)(2,1)S(1)} collective-permute-done((bf16[256,2048]{1,0:T(8,128)(2,1)S(1)}, bf16[256,2048]{1,0:T(8,128)(2,1)S(1)}, u32[]{:S(2)}, u32[]{:S(2)}) %collective-permute-start.3) | collective-permute-done | bytes 1048608 | tf_op jit(solution)/shard_map/ppermute | solution.py:34
  181.7 23.0 %collective-permute-done.5 = bf16[256,2048]{1,0:T(8,128)(2,1)S(1)} collective-permute-done((bf16[256,2048]{1,0:T(8,128)(2,1)S(1)}, bf16[256,2048]{1,0:T(8,128)(2,1)S(1)}, u32[]{:S(2)}, u32[]{:S(2)}) %collective-permute-start.5) | collective-permute-done | bytes 1048608 | tf_op jit(solution)/shard_map/ppermute | solution.py:34
  205.4 1.9 collective-permute-done.6
  208.8 52.6 %all-gather.9.cloned.1.call-done = bf16[2048,2048]{1,0:T(8,128)(2,1)} async-done(((bf16[256,2048]{1,0:T(8,128)(2,1)}), bf16[2048,2048]{1,0:T(8,128)(2,1)}) %all-gather.9.cloned.1.call-update) | async-done | bytes 8388624 | tf_op jit(solution)/shard_map/all_gather | solution.py:103
  261.5 13.8 %fusion.10 = f32[1024,2048]{1,0:T(8,128)} fusion(bf16[2048,2048]{1,0:T(8,128)(2,1)} %all-gather.9.cloned.1.call-done, bf16[256,2048]{1,0:T(8,128)(2,1)} %get-tuple-element.15, bf16[256,2048]{1,0:T(8,128)(2,1)} %get-tuple-element.14, bf16[256,2048]{1,0:T(8,128)(2,1)S(1)} %get-tuple-element.13, bf16[256,2048]{1,0:T(8,128)(2,1)S(1)} %get-tuple-element.12), kind=kOutput, calls=%fused_computation.13 | convolution fusion | flops 8606711808 | bytes 20971520 | tf_op jit(solution)/shard_map/dot_general | solution.py:117
  275.3 60.9 %all-gather.11.cloned.1.call-done = bf16[1024,2048]{1,0:T(8,128)(2,1)} async-done(((bf16[1024,256]{1,0:T(8,128)(2,1)}), bf16[1024,2048]{1,0:T(8,128)(2,1)}) %all-gather.11.cloned.1.call-update) | async-done | bytes 4194320 | tf_op jit(solution)/shard_map/all_gather | solution.py:104
  336.2 9.2 %convolution_convert_fusion.1 = bf16[1024,2048]{1,0:T(8,128)(2,1)S(1)} fusion(bf16[1024,2048]{1,0:T(8,128)(2,1)} %all-gather.11.cloned.1.call-done, f32[1024,2048]{1,0:T(8,128)} %fusion.10), kind=kOutput, calls=%fused_computation.25 | convolution fusion | flops 4303355904 | bytes 16777216 | tf_op jit(solution)/shard_map/dot_general | solution.py:121
  345.6 4.1 %collective-permute-done.7 = bf16[2,256,2048]{2,1,0:T(8,128)(2,1)S(1)} collective-permute-done((bf16[2,256,2048]{2,1,0:T(8,128)(2,1)S(1)}, bf16[2,256,2048]{2,1,0:T(8,128)(2,1)S(1)}, u32[]{:S(2)}, u32[]{:S(2)}) %collective-permute-start.7) | collective-permute-done | bytes 2097184 | tf_op jit(solution)/shard_map/ppermute | solution.py:34
  350.7 1.6 collective-permute-start.8
  352.3 23.7 %collective-permute-done.8 = bf16[256,2048]{1,0:T(8,128)(2,1)S(1)} collective-permute-done((bf16[256,2048]{1,0:T(8,128)(2,1)S(1)}, bf16[256,2048]{1,0:T(8,128)(2,1)S(1)}, u32[]{:S(2)}, u32[]{:S(2)}) %collective-permute-start.8) | collective-permute-done | bytes 1048608 | tf_op jit(solution)/shard_map/ppermute | solution.py:34
  376.5 2.6 collective-permute-done.9
  379.3 1.6 pad_maximum_fusion
  (64 shorter events, 20.7 us)
Async XLA Ops:
  6.5 139.7 %copy-start = (bf16[2048,256]{1,0:T(8,128)(2,1)S(1)}, bf16[2048,256]{1,0:T(8,128)(2,1)}, u32[]{:S(2)}) copy-start(bf16[2048,256]{1,0:T(8,128)(2,1)} %param.21) | copy-start | bytes 3145732
  6.5 3.1 copy-start.6
  6.5 85.3 %all-gather.5.cloned.1.call-start = ((), (), s32[]{:S(2)}) async-start(), calls=%async_computation | async-start | bytes 5308416 | tf_op jit(solution)/shard_map/all_gather | solution.py:100
  9.6 127.1 %all-gather.7.cloned.1.call-start = ((), (), s32[]{:S(2)}) async-start(), calls=%async_computation.1 | async-start | bytes 1769472 | tf_op jit(solution)/shard_map/all_gather | solution.py:101
  10.4 251.1 %all-gather.9.cloned.1.call-start = ((), (), s32[]{:S(2)}) async-start(), calls=%async_computation.2 | async-start | bytes 9437184 | tf_op jit(solution)/shard_map/all_gather | solution.py:103
  10.4 2.6 copy-start.7
  10.4 2.6 copy-start.2
  13.0 323.2 %all-gather.11.cloned.1.call-start = ((), (), s32[]{:S(2)}) async-start(), calls=%async_computation.3 | async-start | bytes 4718592 | tf_op jit(solution)/shard_map/all_gather | solution.py:104
  13.6 28.3 %copy-start.9 = (bf16[3,768]{1,0:T(4,128)(2,1)S(1)}, bf16[3,768]{1,0:T(4,128)(2,1)}, u32[]{:S(2)}) copy-start(bf16[3,768]{1,0:T(4,128)(2,1)} %param.16) | copy-start | bytes 13828
  14.1 1.3 copy-start.3
  15.6 26.3 %collective-permute-start = (bf16[256,2048]{1,0:T(8,128)(2,1)S(1)}, bf16[256,2048]{1,0:T(8,128)(2,1)}, u32[]{:S(2)}, u32[]{:S(2)}) collective-permute-start(bf16[256,2048]{1,0:T(8,128)(2,1)S(1)} %constant_dynamic-slice_fusion.8), channel_id=1, source_target_pairs={{0,16},{16,0},{1,17},{17,1},{2,18},{18,2},{3,19},{19,3},{4,20},{20... | collective-permute-start | bytes 3145736 | tf_op jit(solution)/shard_map/ppermute | solution.py:34
  41.9 3.0 collective-permute-start.1
  101.6 1.5 copy-start.5
  142.7 2.0 copy-start.4
  146.2 4.5 %collective-permute-start.2 = (bf16[2,256,2048]{2,1,0:T(8,128)(2,1)}, bf16[2,256,2048]{2,1,0:T(8,128)(2,1)}, u32[]{:S(2)}, u32[]{:S(2)}) collective-permute-start(bf16[2,256,2048]{2,1,0:T(8,128)(2,1)} %dynamic-slice_bitcast_fusion.1), channel_id=1, source_target_pairs={{0,1},{1,0},{2,3},{3,2},{4,5},{5,4},{6,7},{7,6},{8,9},{9,8},{10,11... | collective-permute-start | bytes 6291464 | tf_op jit(solution)/shard_map/ppermute | solution.py:34
  147.1 8.4 %copy-start.8 = (bf16[2048]{0:T(1024)(128)(2,1)S(1)}, bf16[2048]{0:T(1024)(128)(2,1)}, u32[]{:S(2)}) copy-start(bf16[2048]{0:T(1024)(128)(2,1)} %param.18) | copy-start | bytes 12292
  153.9 25.3 %collective-permute-start.3 = (bf16[256,2048]{1,0:T(8,128)(2,1)S(1)}, bf16[256,2048]{1,0:T(8,128)(2,1)S(1)}, u32[]{:S(2)}, u32[]{:S(2)}) collective-permute-start(bf16[256,2048]{1,0:T(8,128)(2,1)S(1)} %fusion.31), channel_id=1, source_target_pairs={{0,16},{16,0},{1,17},{17,1},{2,18},{18,2},{3,19},{19,3},{4,20},{20... | collective-permute-start | bytes 3145736 | tf_op jit(solution)/shard_map/ppermute | solution.py:34
  180.2 24.5 %collective-permute-start.5 = (bf16[256,2048]{1,0:T(8,128)(2,1)S(1)}, bf16[256,2048]{1,0:T(8,128)(2,1)S(1)}, u32[]{:S(2)}, u32[]{:S(2)}) collective-permute-start(bf16[256,2048]{1,0:T(8,128)(2,1)S(1)} %fusion.23), channel_id=1, source_target_pairs={{0,16},{16,0},{1,17},{17,1},{2,18},{18,2},{3,19},{19,3},{4,20},{20... | collective-permute-start | bytes 3145736 | tf_op jit(solution)/shard_map/ppermute | solution.py:34
  181.7 23.0 %collective-permute-start.4 = (bf16[256,2048]{1,0:T(8,128)(2,1)S(1)}, bf16[256,2048]{1,0:T(8,128)(2,1)S(1)}, u32[]{:S(2)}, u32[]{:S(2)}) collective-permute-start(bf16[256,2048]{1,0:T(8,128)(2,1)S(1)} %fusion.23), channel_id=1, source_target_pairs={{0,1},{1,0},{2,3},{3,2},{4,5},{5,4},{6,7},{7,6},{8,9},{9,8},{10,11... | collective-permute-start | bytes 3145736 | tf_op jit(solution)/shard_map/ppermute | solution.py:34
  204.7 2.7 collective-permute-start.6
  345.6 4.2 %collective-permute-start.7 = (bf16[2,256,2048]{2,1,0:T(8,128)(2,1)S(1)}, bf16[2,256,2048]{2,1,0:T(8,128)(2,1)S(1)}, u32[]{:S(2)}, u32[]{:S(2)}) collective-permute-start(bf16[2,256,2048]{2,1,0:T(8,128)(2,1)S(1)} %dynamic-slice_bitcast_fusion), channel_id=1, source_target_pairs={{0,1},{1,0},{2,3},{3,2},{4,5},{5,4},{6,7},{7,6},{8,9},{9,8},{10,11... | collective-permute-start | bytes 6291464 | tf_op jit(solution)/shard_map/ppermute | solution.py:34
  350.7 25.3 %collective-permute-start.8 = (bf16[256,2048]{1,0:T(8,128)(2,1)S(1)}, bf16[256,2048]{1,0:T(8,128)(2,1)S(1)}, u32[]{:S(2)}, u32[]{:S(2)}) collective-permute-start(bf16[256,2048]{1,0:T(8,128)(2,1)S(1)} %fusion.32), channel_id=1, source_target_pairs={{0,16},{16,0},{1,17},{17,1},{2,18},{18,2},{3,19},{19,3},{4,20},{20... | collective-permute-start | bytes 3145736 | tf_op jit(solution)/shard_map/ppermute | solution.py:34
  376.5 2.7 collective-permute-start.9
  379.2 1.7 copy-start.1
Sparse Core Ops, SparseCore 0:
  9.7 82.0 all-gather.4
  93.8 42.7 all-gather.6
  138.8 122.6 all-gather.8
  263.4 72.8 all-gather.10

commit v2 on v1

--- a/solution.py
+++ b/solution.py
@@ -1,6 +1,8 @@
 import jax
 import jax.numpy as jnp
 from jax import lax
+from jax.experimental import pallas as pl
+from jax.experimental.pallas import tpu as pltpu
 from jax.sharding import PartitionSpec as P
 
 SEQ_GRP = 2
@@ -47,6 +49,127 @@
     return whole
 
 
+WIDTH = 2
+LONGEST_LINE = 4
+
+
+def gather_kernel(depth, block_ref, whole_ref, send_sems, recv_sems, own_sem):
+    me = lax.axis_index("fs")
+    place, side = me // WIDTH, me % WIDTH
+    rows = block_ref.shape[0]
+
+    def slot(source_place, source_side):
+        start = (source_place * WIDTH + source_side) * rows
+        return whole_ref.at[pl.ds(pl.multiple_of(start, 16), rows), :]
+
+    def copy(kind, step, source_place, to_place, to_side, first, source_side=None):
+        landing = slot(source_place, side if source_side is None else source_side)
+        return pltpu.make_async_remote_copy(
+            src_ref=block_ref if first else landing,
+            dst_ref=landing,
+            send_sem=send_sems.at[kind, step],
+            recv_sem=recv_sems.at[kind, step],
+            device_id={"fs": to_place * WIDTH + to_side},
+            device_id_type=pl.DeviceIdType.MESH,
+        )
+
+    def up(step):
+        return copy(0, step, place - (step - 1), place + 1, side, step == 1)
+
+    def up_came(step):
+        return copy(0, step, place - step, place, 1 - side, False)
+
+    def down(step):
+        return copy(1, step, place + (step - 1), place - 1, side, step == 1)
+
+    def down_came(step):
+        return copy(1, step, place + step, place, 1 - side, False)
+
+    def over(kind, step):
+        source = place - step if kind == 2 else place + step
+        return copy(kind, step, source, place, 1 - side, step == 0)
+
+    def over_came(kind, step):
+        source = place - step if kind == 2 else place + step
+        return copy(kind, step, source, place, 1 - side, False, 1 - side)
+
+    has_up, has_down = place < depth - 1, place > 0
+
+    barrier = pltpu.get_barrier_semaphore()
+
+    def greet(to):
+        pl.semaphore_signal(
+            barrier, inc=1, device_id={"fs": to}, device_id_type=pl.DeviceIdType.MESH
+        )
+
+    greet(place * WIDTH + 1 - side)
+    pl.when(has_up)(lambda: greet((place + 1) * WIDTH + side))
+    pl.when(has_down)(lambda: greet((place - 1) * WIDTH + side))
+    pl.semaphore_wait(barrier, 1 + has_up.astype(jnp.int32) + has_down.astype(jnp.int32))
+
+    pl.when(has_up)(lambda: up(1).start())
+    pl.when(has_down)(lambda: down(1).start())
+    over(2, 0).start()
+    own = pltpu.make_async_copy(block_ref, slot(place, side), own_sem)
+    own.start()
+
+    for step in range(1, depth):
+
+        @pl.when(place >= step)
+        def _(step=step):
+            up_came(step).wait_recv()
+            if step + 1 < depth:
+                pl.when(has_up)(lambda: up(step + 1).start())
+            over(2, step).start()
+
+        @pl.when(place + step < depth)
+        def _(step=step):
+            down_came(step).wait_recv()
+            if step + 1 < depth:
+                pl.when(has_down)(lambda: down(step + 1).start())
+            over(3, step).start()
+
+    own.wait()
+    over(2, 0).wait_send()
+    over_came(2, 0).wait_recv()
+    for step in range(1, depth):
+        pl.when((place >= step - 1) & has_up)(lambda step=step: up(step).wait_send())
+        pl.when((place + step - 1 < depth) & has_down)(lambda step=step: down(step).wait_send())
+
+        @pl.when(place >= step)
+        def _(step=step):
+            over(2, step).wait_send()
+            over_came(2, step).wait_recv()
+
+        @pl.when(place + step < depth)
+        def _(step=step):
+            over(3, step).wait_send()
+            over_came(3, step).wait_recv()
+
+
+def gather_fs(block):
+    size = lax.axis_size("fs")
+    depth = size // WIDTH
+    rows, cols = block.shape
+    if size % WIDTH or depth > LONGEST_LINE or rows % 16 or cols % 128:
+        return lax.all_gather(block, "fs", axis=0, tiled=True)
+    moved = size * rows * cols * 2
+    return pl.pallas_call(
+        lambda *refs: gather_kernel(depth, *refs),
+        out_shape=jax.ShapeDtypeStruct((size * rows, cols), block.dtype),
+        in_specs=[pl.BlockSpec(memory_space=pl.ANY)],
+        out_specs=pl.BlockSpec(memory_space=pl.ANY),
+        scratch_shapes=[
+            pltpu.SemaphoreType.DMA((4, depth)),
+            pltpu.SemaphoreType.DMA((4, depth)),
+            pltpu.SemaphoreType.DMA,
+        ],
+        compiler_params=pltpu.CompilerParams(collective_id=0, has_side_effects=True),
+        cost_estimate=pl.CostEstimate(flops=0, bytes_accessed=40 * moved, transcendentals=0),
+        name="gather_mixer_weights",
+    )(block)
+
+
 def by_rep(block):
     return [block] + [shifted(block, "rep", step) for step in range(1, lax.axis_size("rep"))]
 
@@ -69,6 +192,12 @@
     for step in range(1, n_rep):
         own = own + shifted(total[step].astype(jnp.bfloat16), "rep", -step).astype(jnp.float32)
     return own
+
+
+def dot_t(left, right):
+    return lax.dot_general(
+        left, right, (((1,), (1,)), ((), ())), preferred_element_type=jnp.float32
+    )
 
 
 def local(
@@ -94,23 +223,27 @@
         return lax.dynamic_slice_in_dim(array, rep * size, size, axis)
 
     own_tokens = lax.dynamic_slice_in_dim(tokens, lax.axis_index("tp") * share, share, 0)
-    conv_in = jnp.concatenate(
-        [part(w, 1) for w in (value_weight, outer_gate_weight, inner_gate_weight)], axis=1
-    )
-    conv_full = lax.all_gather(conv_in, "fs", axis=0, tiled=True)
-    mix_out_full = lax.all_gather(part(mix_out_weight, 0), "fs", axis=1, tiled=True)
+    mix_in = jnp.concatenate(
+        [part(w, 1) for w in (value_weight, outer_gate_weight, inner_gate_weight)]
+        + [part(mix_out_weight, 0).T],
+        axis=1,
+    )
+    mix_full = gather_fs(mix_in)
+    channels = mix_out_weight.shape[0] // n_rep
     ffn_in = jnp.concatenate([part(w, 1) for w in (gate_weight, up_weight)], axis=1)
     ffn_full = lax.all_gather(ffn_in, "fs", axis=0, tiled=True)
     down_full = lax.all_gather(part(down_weight, 0), "fs", axis=1, tiled=True)
 
     normed = rms_norm(tokens, mix_gain)
     own_normed = lax.dynamic_slice_in_dim(normed, lax.axis_index("tp") * share, share, 0)
-    rows = jnp.concatenate([normed] + [spread(b, "tp") for b in by_rep(own_normed)[1:]])
+    received, mix_full = lax.optimization_barrier((by_rep(own_normed)[1:], mix_full))
+    conv_full, mix_out_full = mix_full[:, : 3 * channels], mix_full[:, 3 * channels :]
+    rows = jnp.concatenate([normed] + [spread(b, "tp") for b in received])
     proj = jnp.dot(rows, conv_full, preferred_element_type=jnp.float32).astype(jnp.bfloat16)
     value_proj, outer_proj, inner_proj = jnp.split(proj, 3, axis=1)
     mixed = short_conv(value_proj, outer_proj, inner_proj, part(conv_taps, 1), seq_len)
     mix_total = reduce_rows(
-        jnp.dot(mixed, mix_out_full, preferred_element_type=jnp.float32).astype(jnp.bfloat16), share
+        dot_t(mixed, mix_out_full).astype(jnp.bfloat16), share
     )
     after_mix = (own_tokens.astype(jnp.float32) + mix_total).astype(jnp.bfloat16)
     block_rows = group_rows(rms_norm(after_mix, ffn_gain))

time: 388 us -> 321 us (0.83)
  waiting for transfers between devices: 299 us -> 88 us
  Pallas kernels: 0 us -> 149 us
    pallas_call x0 -> x1, Pallas kernels: none -> 149 us  [gather_fs(): pl.pallas_call(lambda *refs: gather_kernel(depth, *refs), out_shape=jax.S...]
    all_gather x2 -> x0, waiting for transfers between devices: 76.1 us -> none  [the longest x1 43.9 us: local(): conv_full = lax.all_gather(conv_in, 'fs', axis=0, tiled=True)]
    all_gather x1, waiting for transfers between devices: 60.9 us -> 0.01 us  [local(): down_full = lax.all_gather(part(down_weight, 0), 'fs', axis=1, tiled=True)]
    all_gather x1, waiting for transfers between devices: 52.6 us -> 0.01 us  [local(): ffn_full = lax.all_gather(ffn_in, 'fs', axis=0, tiled=True)]
    ppermute x10, waiting for transfers between devices: 109 us -> 87.9 us  [shifted(): lax.ppermute(values, axis, [(i, (i + step) % size) for i in range(size)])]
  transfers between devices with their start and end apart: 14 -> 12, of which waited for: 13 -> 8; matrix products, arithmetic and copies ran while one was open for 12% -> 15% of each run, Pallas kernels for 0% -> 46%
where the time goes in v2:
time: 321 us
  Pallas kernels  149 us (46%)
  waiting for transfers between devices  88 us (27%)
  matrix products  38.9 us (12%)
  other arithmetic  15.1 us (5%)
  between operations  13.7 us (4%)
  local copies, waits for them, and re-layouts  11.6 us (4%)
  starting transfers between devices  4.55 us (1%)
    pallas_call x1, Pallas kernels, gather_fs(): pl.pallas_call(lambda *refs: gather_kernel(depth, *refs), out_shape=jax.S...  149 us
    ppermute x10, waiting for transfers between devices, shifted(): lax.ppermute(values, axis, [(i, (i + step) % size) for i in range(size)])  87.9 us
    dot_general x1, matrix products, local(): both = jnp.dot(block_rows, ffn_full, preferred_element_type=jnp.float32)  14.2 us
    dot_general x1, matrix products, local(): jnp.dot(rows, conv_full, preferred_element_type=jnp.float32)  10.5 us
    dot_general x1, matrix products, local(): jnp.dot(hidden, down_full, preferred_element_type=jnp.float32)  9.2 us
  transfers between devices with their start and end apart: 12, of which 8 were waited for; matrix products, arithmetic and copies ran while one was open for 15% of the time, Pallas kernels for 46%

profile of v2, /device:TPU:0, one launch (start us, length us, event | category | flops | bytes accessed | tf_op | source)
XLA Modules:
  0.0 320.8 jit_solution(16581001736507315405)
XLA Ops:
  6.5 1.4 constant_dynamic-slice_fusion.1
  8.0 1.1 pad_maximum_fusion.1
  10.2 1.3 copy-done.3
  12.6 3.0 collective-permute-start
  17.6 1.1 constant_dynamic-slice_fusion.5
  19.7 149.0 %gather_mixer_weights.1 = bf16[2048,1536]{1,0:T(8,128)(2,1)} custom-call(bf16[256,1536]{1,0:T(8,128)(2,1)} %pad_maximum_fusion.2.refs_0_), custom_call_target="tpu_custom_call" | custom-call | bytes 251658240 | tf_op jit(solution)/shard_map/gather_mixer_weights/pallas_call | solution.py:157
  168.8 2.9 collective-permute-done.1
  171.7 1.7 broadcast_select_fusion.7
  173.4 10.5 %fusion.19 = bf16[1024,1152]{1,0:T(8,128)(2,1)S(1)} fusion(bf16[2048,1536]{1,0:T(8,128)(2,1)} %gather_mixer_weights.1, bf16[256,2048]{1,0:T(8,128)(2,1)S(1)} %get-tuple-element.21, bf16[256,2048]{1,0:T(8,128)(2,1)S(1)} %get-tuple-element.20, bf16[512,2048]{1,0:T(8,128)(2,1)S(1)} %copy-done.4), kind=kOutput, calls=%fused_computation.25 | convolution fusion | flops 4845600768 | bytes 11272192 | tf_op jit(solution)/shard_map/dot_general | solution.py:242
  184.1 5.1 %convolution_convert_fusion = bf16[1024,2048]{1,0:T(8,128)(2,1)S(1)} fusion(bf16[2048,1536]{1,0:T(8,128)(2,1)} %gather_mixer_weights.1, f32[1023,384]{1,0:T(8,128)S(1)} %bitcast.44, f32[1022,384]{1,0:T(8,128)S(1)} %bitcast.45, bf16[1024,1152]{1,0:T(8,128)(2,1)S(1)} %fusion.19, f32[384]{0:T(512)S(1)} %get-tuple-element.10, f32[384]{0:T(512)S(1)} %get-tuple-element.11, ...), kind=kOutput, calls=%fused_computation.24 | convolution fusion | flops 1617821696 | bytes 11274240 | tf_op jit(solution)/shard_map/dot_general | solution.py:198
  189.2 2.0 copy-done.5
  191.1 1.5 dynamic-slice_bitcast_fusion.1
  193.6 3.5 %collective-permute-done.2 = bf16[2,256,2048]{2,1,0:T(8,128)(2,1)} collective-permute-done((bf16[2,256,2048]{2,1,0:T(8,128)(2,1)}, bf16[2,256,2048]{2,1,0:T(8,128)(2,1)}, u32[]{:S(2)}, u32[]{:S(2)}) %collective-permute-start.2) | collective-permute-done | bytes 2097184 | tf_op jit(solution)/shard_map/ppermute | solution.py:36
  197.1 3.0 convert_add_fusion.1
  200.4 25.2 %collective-permute-done.3 = bf16[256,2048]{1,0:T(8,128)(2,1)S(1)} collective-permute-done((bf16[256,2048]{1,0:T(8,128)(2,1)S(1)}, bf16[256,2048]{1,0:T(8,128)(2,1)S(1)}, u32[]{:S(2)}, u32[]{:S(2)}) %collective-permute-start.3) | collective-permute-done | bytes 1048608 | tf_op jit(solution)/shard_map/ppermute | solution.py:36
  226.8 24.2 %collective-permute-done.5 = bf16[256,2048]{1,0:T(8,128)(2,1)S(1)} collective-permute-done((bf16[256,2048]{1,0:T(8,128)(2,1)S(1)}, bf16[256,2048]{1,0:T(8,128)(2,1)S(1)}, u32[]{:S(2)}, u32[]{:S(2)}) %collective-permute-start.5) | collective-permute-done | bytes 1048608 | tf_op jit(solution)/shard_map/ppermute | solution.py:36
  251.0 1.7 broadcast_select_fusion.5
  253.7 1.5 broadcast_select_fusion.3
  255.1 14.2 %fusion.11 = f32[1024,2048]{1,0:T(8,128)} fusion(bf16[2048,2048]{1,0:T(8,128)(2,1)} %all-gather.3.cloned.1.call-done, bf16[256,2048]{1,0:T(8,128)(2,1)} %get-tuple-element.19, bf16[256,2048]{1,0:T(8,128)(2,1)} %get-tuple-element.18, bf16[256,2048]{1,0:T(8,128)(2,1)} %get-tuple-element.17, bf16[256,2048]{1,0:T(8,128)(2,1)S(1)} %get-tuple-element.16), kind=kOutput, calls=%fused_computation.14 | convolution fusion | flops 8606711808 | bytes 20971520 | tf_op jit(solution)/shard_map/dot_general | solution.py:250
  269.3 9.2 %convolution_convert_fusion.1 = bf16[1024,2048]{1,0:T(8,128)(2,1)S(1)} fusion(bf16[1024,2048]{1,0:T(8,128)(2,1)} %all-gather.5.cloned.1.call-done, f32[1024,2048]{1,0:T(8,128)} %fusion.11), kind=kOutput, calls=%fused_computation.26 | convolution fusion | flops 4303355904 | bytes 16777216 | tf_op jit(solution)/shard_map/dot_general | solution.py:254
  278.8 4.0 %collective-permute-done.7 = bf16[2,256,2048]{2,1,0:T(8,128)(2,1)S(1)} collective-permute-done((bf16[2,256,2048]{2,1,0:T(8,128)(2,1)S(1)}, bf16[2,256,2048]{2,1,0:T(8,128)(2,1)S(1)}, u32[]{:S(2)}, u32[]{:S(2)}) %collective-permute-start.7) | collective-permute-done | bytes 2097184 | tf_op jit(solution)/shard_map/ppermute | solution.py:36
  284.4 24.6 %collective-permute-done.8 = bf16[256,2048]{1,0:T(8,128)(2,1)S(1)} collective-permute-done((bf16[256,2048]{1,0:T(8,128)(2,1)S(1)}, bf16[256,2048]{1,0:T(8,128)(2,1)S(1)}, u32[]{:S(2)}, u32[]{:S(2)}) %collective-permute-start.8) | collective-permute-done | bytes 1048608 | tf_op jit(solution)/shard_map/ppermute | solution.py:36
  309.6 2.6 collective-permute-done.9
  312.4 1.6 pad_maximum_fusion
  (58 shorter events, 11.5 us)
Async XLA Ops:
  6.5 186.2 %copy-start = (bf16[2048,256]{1,0:T(8,128)(2,1)S(1)}, bf16[2048,256]{1,0:T(8,128)(2,1)}, u32[]{:S(2)}) copy-start(bf16[2048,256]{1,0:T(8,128)(2,1)} %param.21) | copy-start | bytes 3145732
  6.5 248.6 %all-gather.3.cloned.1.call-start = ((), (), s32[]{:S(2)}) async-start(), calls=%async_computation | async-start | bytes 9437184 | tf_op jit(solution)/shard_map/all_gather | solution.py:234
  6.5 2.6 copy-start.6
  6.5 2.6 copy-start.2
  9.1 260.2 %all-gather.5.cloned.1.call-start = ((), (), s32[]{:S(2)}) async-start(), calls=%async_computation.1 | async-start | bytes 4718592 | tf_op jit(solution)/shard_map/all_gather | solution.py:235
  10.2 1.3 copy-start.3
  12.6 156.1 %collective-permute-start = (bf16[256,2048]{1,0:T(8,128)(2,1)}, bf16[256,2048]{1,0:T(8,128)(2,1)}, u32[]{:S(2)}, u32[]{:S(2)}) collective-permute-start(bf16[256,2048]{1,0:T(8,128)(2,1)} %constant_dynamic-slice_fusion.8), channel_id=1, source_target_pairs={{0,16},{16,0},{1,17},{17,1},{2,18},{18,2},{3,19},{19,3},{4,20},{20... | collective-permute-start | bytes 3145736 | tf_op jit(solution)/shard_map/ppermute | solution.py:36
  19.7 149.1 %copy-start.8 = (bf16[3,768]{1,0:T(4,128)(2,1)S(1)}, bf16[3,768]{1,0:T(4,128)(2,1)}, u32[]{:S(2)}) copy-start(bf16[3,768]{1,0:T(4,128)(2,1)} %param.16) | copy-start | bytes 13828
  168.7 3.1 collective-permute-start.1
  168.8 4.7 %copy-start.4 = (bf16[512,2048]{1,0:T(8,128)(2,1)S(1)}, bf16[512,2048]{1,0:T(8,128)(2,1)}, u32[]{:S(2)}) copy-start(bf16[512,2048]{1,0:T(8,128)(2,1)} %copy-done.3) | copy-start | bytes 6291460
  189.2 2.0 copy-start.5
  192.6 4.5 %collective-permute-start.2 = (bf16[2,256,2048]{2,1,0:T(8,128)(2,1)}, bf16[2,256,2048]{2,1,0:T(8,128)(2,1)}, u32[]{:S(2)}, u32[]{:S(2)}) collective-permute-start(bf16[2,256,2048]{2,1,0:T(8,128)(2,1)} %dynamic-slice_bitcast_fusion.1), channel_id=1, source_target_pairs={{0,1},{1,0},{2,3},{3,2},{4,5},{5,4},{6,7},{7,6},{8,9},{9,8},{10,11... | collective-permute-start | bytes 6291464 | tf_op jit(solution)/shard_map/ppermute | solution.py:36
  193.6 6.8 %copy-start.7 = (bf16[2048]{0:T(1024)(128)(2,1)S(1)}, bf16[2048]{0:T(1024)(128)(2,1)}, u32[]{:S(2)}) copy-start(bf16[2048]{0:T(1024)(128)(2,1)} %param.18) | copy-start | bytes 12292
  200.3 25.3 %collective-permute-start.3 = (bf16[256,2048]{1,0:T(8,128)(2,1)S(1)}, bf16[256,2048]{1,0:T(8,128)(2,1)S(1)}, u32[]{:S(2)}, u32[]{:S(2)}) collective-permute-start(bf16[256,2048]{1,0:T(8,128)(2,1)S(1)} %fusion.35), channel_id=1, source_target_pairs={{0,16},{16,0},{1,17},{17,1},{2,18},{18,2},{3,19},{19,3},{4,20},{20... | collective-permute-start | bytes 3145736 | tf_op jit(solution)/shard_map/ppermute | solution.py:36
  226.5 24.5 %collective-permute-start.5 = (bf16[256,2048]{1,0:T(8,128)(2,1)S(1)}, bf16[256,2048]{1,0:T(8,128)(2,1)S(1)}, u32[]{:S(2)}, u32[]{:S(2)}) collective-permute-start(bf16[256,2048]{1,0:T(8,128)(2,1)S(1)} %fusion.26), channel_id=1, source_target_pairs={{0,16},{16,0},{1,17},{17,1},{2,18},{18,2},{3,19},{19,3},{4,20},{20... | collective-permute-start | bytes 3145736 | tf_op jit(solution)/shard_map/ppermute | solution.py:36
  226.8 24.2 %collective-permute-start.4 = (bf16[256,2048]{1,0:T(8,128)(2,1)S(1)}, bf16[256,2048]{1,0:T(8,128)(2,1)S(1)}, u32[]{:S(2)}, u32[]{:S(2)}) collective-permute-start(bf16[256,2048]{1,0:T(8,128)(2,1)S(1)} %fusion.26), channel_id=1, source_target_pairs={{0,1},{1,0},{2,3},{3,2},{4,5},{5,4},{6,7},{7,6},{8,9},{9,8},{10,11... | collective-permute-start | bytes 3145736 | tf_op jit(solution)/shard_map/ppermute | solution.py:36
  251.0 2.7 collective-permute-start.6
  278.7 4.2 %collective-permute-start.7 = (bf16[2,256,2048]{2,1,0:T(8,128)(2,1)S(1)}, bf16[2,256,2048]{2,1,0:T(8,128)(2,1)S(1)}, u32[]{:S(2)}, u32[]{:S(2)}) collective-permute-start(bf16[2,256,2048]{2,1,0:T(8,128)(2,1)S(1)} %dynamic-slice_bitcast_fusion), channel_id=1, source_target_pairs={{0,1},{1,0},{2,3},{3,2},{4,5},{5,4},{6,7},{7,6},{8,9},{9,8},{10,11... | collective-permute-start | bytes 6291464 | tf_op jit(solution)/shard_map/ppermute | solution.py:36
  283.8 25.3 %collective-permute-start.8 = (bf16[256,2048]{1,0:T(8,128)(2,1)S(1)}, bf16[256,2048]{1,0:T(8,128)(2,1)S(1)}, u32[]{:S(2)}, u32[]{:S(2)}) collective-permute-start(bf16[256,2048]{1,0:T(8,128)(2,1)S(1)} %fusion.36), channel_id=1, source_target_pairs={{0,16},{16,0},{1,17},{17,1},{2,18},{18,2},{3,19},{19,3},{4,20},{20... | collective-permute-start | bytes 3145736 | tf_op jit(solution)/shard_map/ppermute | solution.py:36
  309.6 2.7 collective-permute-start.9
  312.3 1.7 copy-start.1
Sparse Core Ops, SparseCore 0:
  9.5 175.9 all-gather.2
  193.7 73.8 all-gather.4
